TPU v7x, 32 devices: a whole 2x2x4 slice. The times are simulated.
32 devices in a mesh: sp: 8 (over z, x), tp: 4 (over y, core).
Axes of the slice: x: 2, y: 2, z: 4, core: 2. Of those that a mesh axis runs over, the one named last changes fastest.
Arguments:
- resid: bfloat16 [1024, 2048], P('sp'), may hold values from -6 to 6
- norm_gain: float32 [2048], replicated, may hold values from 0.1 to 1.9
- cotangent: bfloat16 [1024, 2048], P('sp'), may hold values from -6 to 6
- route_ids: int32 [1024, 2], P('sp'), may hold values from 0 to 7, all different within a row; in each aligned block of 128 rows (0 to 127, 128 to 255, ...) at most 48 rows name the same one
- route_weight: float32 [1024, 2], P('sp'), may hold values from 0.25 to 2.25
- expert_gate: bfloat16 [8, 2048, 2048], P('sp', None, 'tp'), may hold values from -0.125 to 0.125
- expert_up: bfloat16 [8, 2048, 2048], P('sp', None, 'tp'), may hold values from -0.125 to 0.125
- expert_down: bfloat16 [8, 2048, 2048], P('sp', 'tp'), may hold values from -0.125 to 0.125
- out_proj: bfloat16 [2048, 4096], P('sp', 'tp'), may hold values from -0.09375 to 0.09375
- mixed: bfloat16 [1024, 4096], P('sp', 'tp'), may hold values from -6 to 6
- query: bfloat16 [1024, 2048], P('sp', 'tp'), may hold values from -6 to 6
- key: bfloat16 [1024, 2048], P('sp', 'tp'), may hold values from -1.5 to 1.5
- value: bfloat16 [1024, 4096], P('sp', 'tp'), may hold values from -6 to 6
- log_decay: float32 [1024, 2048], P('sp', 'tp'), may hold values from -1 to 0, as said below
- span_state: float32 [8, 16, 128, 256], P('sp', 'tp'), may hold values from -24 to 24
Outputs:
- grad_expert_gate: bfloat16 [8, 2048, 2048], P('sp', None, 'tp')
- grad_expert_up: bfloat16 [8, 2048, 2048], P('sp', None, 'tp')
- grad_expert_down: bfloat16 [8, 2048, 2048], P('sp', 'tp')
- grad_out_proj: float32 [2048, 4096], P('sp', 'tp')
- grad_query: bfloat16 [1024, 2048], P('sp', 'tp')
- grad_key: bfloat16 [1024, 2048], P('sp', 'tp')
- grad_value: bfloat16 [1024, 4096], P('sp', 'tp')
- grad_log_decay: float32 [1024, 2048], P('sp', 'tp')
Inputs may be any that keep to these rules, and one draw needn't show every extreme that they name: `route_ids`: A row names 2 different experts. Within each aligned block of 128 rows (the rows of one index of sp) no expert is named by more than 48 rows, and in every draw some expert is named by exactly 48 rows of some block. `log_decay`: every entry is zero or negative.
All inputs are finite; a program needn't handle non-finite values.
Results may differ from a plain program's by a relative error of at most 0.023.
Values may be sent and summed in bfloat16 or wider, within the bound.
A program may use at most 128 MiB of HBM per device.

v0:
```python
import jax
import jax.numpy as jnp
from jax import lax
from jax.sharding import PartitionSpec as P

KEY_CHANNELS = 128
DV = 256
TOP = 2
BLOCK = 64
epsilon = 1e-06
highest = lax.Precision.HIGHEST


def entering(array, axis, join, neutral):
    count = lax.axis_size(axis)
    place = lax.axis_index(axis)
    ahead = count - 1 - place
    gathered = jax.tree.map(
        lambda a, kind: lax.all_gather(a.astype(kind), axis), array, (jnp.bfloat16, jnp.bfloat16)
    )
    state = jax.tree.map(lambda a, e: jnp.zeros_like(a) + jnp.asarray(e, a.dtype), array, neutral)

    def one(lap, state):
        source = count - 1 - lap
        return join(
            state,
            jax.tree.map(
                lambda a, own: lax.dynamic_index_in_dim(a, source, 0, False).astype(own.dtype),
                gathered,
                array,
            ),
        )

    return lax.fori_loop(0, ahead, one, state)


def into_blocks(values):
    return values.reshape(values.shape[0] // BLOCK, BLOCK, values.shape[1])


def span_forward(query_rows, key_rows, value_rows, grad_rows, decay_rows, entry_state):
    query_blk = into_blocks(query_rows)
    key_blk = into_blocks(key_rows)
    value_blk = into_blocks(value_rows)
    grad_blk = into_blocks(grad_rows)
    cumlog = jnp.cumsum(into_blocks(decay_rows), axis=1)
    block_total = cumlog[:, -1, :]
    to_end = jnp.exp(block_total[:, None, :] - cumlog)
    inner_part = jnp.einsum("nsd,nsj->ndj", key_blk * to_end, value_blk, precision=highest)

    def forward_step(carry_state, step_item):
        piece_part, block_sum = step_item
        return (jnp.exp(block_sum)[:, None] * carry_state + piece_part, carry_state)

    end_state, starts = lax.scan(forward_step, entry_state, (inner_part, block_total))
    own_part = jnp.einsum("ntd,ntj->ndj", query_blk * jnp.exp(cumlog), grad_blk, precision=highest)

    def backward_step(carry_state, step_item):
        piece_part, block_sum = step_item
        return (jnp.exp(block_sum)[:, None] * carry_state + piece_part, carry_state)

    start_cot, after_cot = lax.scan(
        backward_step, jnp.zeros_like(entry_state), (own_part, block_total), reverse=True
    )
    span_total = jnp.sum(block_total, axis=0)
    later_log = span_total[None, :] - jnp.cumsum(block_total, axis=0)
    return ((cumlog, starts, after_cot, later_log, end_state), (jnp.exp(span_total), start_cot))


def span_backward(query_rows, key_rows, value_rows, grad_rows, kept_terms, exit_cot):
    cumlog, starts, after_cot, later_log, end_state = kept_terms
    query_blk = into_blocks(query_rows)
    key_blk = into_blocks(key_rows)
    value_blk = into_blocks(value_rows)
    grad_blk = into_blocks(grad_rows)
    exit_cots = after_cot + jnp.exp(later_log)[:, :, None] * exit_cot
    causal = jnp.arange(BLOCK)[:, None] >= jnp.arange(BLOCK)[None, :]
    decays = jnp.exp(
        jnp.where(causal[None, :, :, None], cumlog[:, :, None, :] - cumlog[:, None, :, :], -jnp.inf)
    )
    scores = jnp.einsum("ntd,nsd,ntsd->nts", query_blk, key_blk, decays, precision=highest)
    grad_scores = jnp.einsum("ntj,nsj->nts", grad_blk, value_blk, precision=highest)
    grad_query = jnp.exp(cumlog) * jnp.einsum("ntj,ndj->ntd", grad_blk, starts, precision=highest)
    grad_query = grad_query + jnp.einsum(
        "nts,nsd,ntsd->ntd", grad_scores, key_blk, decays, precision=highest
    )
    to_end = jnp.exp(cumlog[:, -1:, :] - cumlog)
    grad_key = jnp.einsum("nts,ntd,ntsd->nsd", grad_scores, query_blk, decays, precision=highest)
    grad_key = grad_key + to_end * jnp.einsum(
        "nsj,ndj->nsd", value_blk, exit_cots, precision=highest
    )
    grad_value = jnp.einsum("nts,ntj->nsj", scores, grad_blk, precision=highest)
    grad_value = grad_value + jnp.einsum(
        "nsd,ndj->nsj", key_blk * to_end, exit_cots, precision=highest
    )
    length = query_rows.shape[0]
    key_width = query_rows.shape[1]
    per_position = (query_blk * grad_query - key_blk * grad_key).reshape(length, key_width)
    grad_log = (
        jnp.flip(jnp.cumsum(jnp.flip(per_position, 0), 0), 0)
        + jnp.sum(end_state * exit_cot, axis=1)[None, :]
    )
    return (
        grad_query.reshape(length, key_width),
        grad_key.reshape(length, key_width),
        grad_value.reshape(length, value_rows.shape[1]),
        grad_log,
    )


def join_later(earlier, later):
    return (earlier[0] * later[0], later[1] + later[0][..., None] * earlier[1])


def on_device(
    resid,
    norm_gain,
    cotangent,
    route_ids,
    route_weight,
    expert_gate,
    expert_up,
    expert_down,
    out_proj,
    mixed,
    query,
    key,
    value,
    log_decay,
    span_state,
):
    tokens_here = resid.shape[0]
    model_width = resid.shape[1]
    sp_count = lax.axis_size("sp")
    tp_count = lax.axis_size("tp")
    experts = sp_count * expert_gate.shape[0]
    capacity = 3 * tokens_here // experts
    resid_f = resid.astype(jnp.float32)
    inverse_rms = lax.rsqrt(jnp.mean(resid_f * resid_f, axis=1, keepdims=True) + epsilon)
    unit_rows = resid_f * inverse_rms
    normed = (unit_rows * norm_gain).astype(jnp.bfloat16)
    pair_expert = route_ids.reshape(-1)
    onehot = (pair_expert[:, None] == jnp.arange(experts, dtype=jnp.int32)[None, :]).astype(
        jnp.int32
    )
    slot_rank = jnp.sum((jnp.cumsum(onehot, axis=0) - onehot) * onehot, axis=1)
    slot_of = pair_expert * capacity + slot_rank
    slot_pairs = slot_of[None, :] == jnp.arange(experts * capacity, dtype=jnp.int32)[:, None]
    slot_tokens = jnp.any(slot_pairs.reshape(experts * capacity, tokens_here, TOP), axis=2).astype(
        jnp.bfloat16
    )
    slot_weight = jnp.sum(jnp.where(slot_pairs, route_weight.reshape(1, -1), 0.0), axis=1)
    column_share = model_width // tp_count
    offset = lax.axis_index("tp") * column_share
    rows_in = jnp.dot(
        slot_tokens,
        lax.dynamic_slice_in_dim(normed, offset, column_share, 1),
        preferred_element_type=jnp.float32,
    ).astype(jnp.bfloat16)
    rows_cot = (
        jnp.dot(
            slot_tokens,
            lax.dynamic_slice_in_dim(cotangent, offset, column_share, 1),
            preferred_element_type=jnp.float32,
        )
        * slot_weight[:, None]
    )
    arrived = (
        lax.all_to_all(
            rows_in.reshape(experts, capacity, -1), "sp", split_axis=0, concat_axis=1, tiled=True
        ),
        lax.all_to_all(
            rows_cot.astype(jnp.bfloat16).reshape(experts, capacity, -1),
            "sp",
            split_axis=0,
            concat_axis=1,
            tiled=True,
        ),
    )
    expert_in, expert_cot = (
        lax.all_gather(arrived[0], "tp", axis=2, tiled=True),
        lax.all_gather(arrived[1], "tp", axis=2, tiled=True),
    )
    gate_pre = jnp.einsum(
        "erd,edf->erf", expert_in, expert_gate, preferred_element_type=jnp.float32
    )
    up_pre = jnp.einsum("erd,edf->erf", expert_in, expert_up, preferred_element_type=jnp.float32)
    gate_sig = jax.nn.sigmoid(gate_pre)
    hidden = (gate_pre * gate_sig * up_pre).astype(jnp.bfloat16)
    grad_hidden = jnp.einsum(
        "erd,efd->erf", expert_cot, expert_down, preferred_element_type=jnp.float32
    )
    grad_up_act = (grad_hidden * gate_pre * gate_sig).astype(jnp.bfloat16)
    grad_gate_act = (grad_hidden * up_pre * gate_sig * (1.0 + gate_pre * (1.0 - gate_sig))).astype(
        jnp.bfloat16
    )
    grad_down_w = jnp.einsum("erf,erd->efd", hidden, expert_cot, preferred_element_type=jnp.float32)
    grad_gate_w = jnp.einsum(
        "erd,erf->edf", expert_in, grad_gate_act, preferred_element_type=jnp.float32
    )
    grad_up_w = jnp.einsum(
        "erd,erf->edf", expert_in, grad_up_act, preferred_element_type=jnp.float32
    )
    partial_value = jnp.einsum(
        "erf,edf->erd", grad_gate_act, expert_gate, preferred_element_type=jnp.float32
    )
    partial_value = partial_value + jnp.einsum(
        "erf,edf->erd", grad_up_act, expert_up, preferred_element_type=jnp.float32
    )
    partial_short = partial_value.astype(jnp.bfloat16)
    summed = (
        lax.psum_scatter(partial_short, "tp", scatter_dimension=2, tiled=True)
        .astype(jnp.float32)
        .astype(jnp.bfloat16)
    )
    returned = lax.all_to_all(summed, "sp", split_axis=1, concat_axis=0, tiled=True)
    flat_rows = returned.reshape(experts * capacity, -1)
    grad_normed = lax.all_gather(
        lax.dot_general(
            slot_tokens, flat_rows, (((0,), (0,)), ((), ())), preferred_element_type=jnp.float32
        ).astype(jnp.bfloat16),
        "tp",
        axis=1,
        tiled=True,
    ).astype(jnp.float32)
    scaled = grad_normed * norm_gain
    grad_resid = cotangent.astype(jnp.float32) + inverse_rms * (
        scaled - unit_rows * jnp.mean(scaled * unit_rows, axis=1, keepdims=True)
    )
    grad_resid = grad_resid.astype(jnp.bfloat16)
    resid_cols = grad_resid
    grad_out_proj = lax.psum_scatter(
        lax.dot_general(
            resid_cols, mixed, (((0,), (0,)), ((), ())), preferred_element_type=jnp.float32
        ).astype(jnp.bfloat16),
        "sp",
        scatter_dimension=0,
        tiled=True,
    ).astype(jnp.float32)
    resid_cols = grad_resid
    grad_mixed = jnp.dot(
        resid_cols,
        lax.all_gather(out_proj, "sp", axis=0, tiled=True),
        preferred_element_type=jnp.float32,
    ).astype(jnp.bfloat16)
    head_count = query.shape[1] // KEY_CHANNELS
    query_scale = KEY_CHANNELS ** (-0.5)

    def heads_first(values, head_depth):
        return values.reshape(tokens_here, head_count, head_depth).transpose(1, 0, 2)

    query_rows = heads_first(query, KEY_CHANNELS).astype(jnp.float32) * query_scale
    key_rows = heads_first(key, KEY_CHANNELS).astype(jnp.float32)
    value_rows = heads_first(value, DV).astype(jnp.float32)
    grad_rows = heads_first(grad_mixed, DV).astype(jnp.float32)
    decay_rows = heads_first(log_decay, KEY_CHANNELS)
    kept_terms, summary = jax.vmap(span_forward)(
        query_rows, key_rows, value_rows, grad_rows, decay_rows, span_state[0]
    )
    identity = (jnp.ones_like(summary[0]), jnp.zeros_like(summary[1]))
    carried = entering((summary[0], summary[1]), "sp", join_later, identity)
    head_grads = jax.vmap(span_backward)(
        query_rows, key_rows, value_rows, grad_rows, kept_terms, carried[1]
    )

    def tokens_first(values):
        return values.transpose(1, 0, 2).reshape(tokens_here, -1)

    grad_query = (tokens_first(head_grads[0]) * query_scale).astype(jnp.bfloat16)
    grad_key = tokens_first(head_grads[1]).astype(jnp.bfloat16)
    grad_value = tokens_first(head_grads[2]).astype(jnp.bfloat16)
    grad_log_decay = tokens_first(head_grads[3])
    return (
        grad_gate_w.astype(jnp.bfloat16),
        grad_up_w.astype(jnp.bfloat16),
        grad_down_w.astype(jnp.bfloat16),
        grad_out_proj,
        grad_query,
        grad_key,
        grad_value,
        grad_log_decay,
    )


def solution(mesh):
    return jax.shard_map(
        on_device,
        mesh=mesh,
        in_specs=(
            P("sp", None),
            P(),
            P("sp", None),
            P("sp", None),
            P("sp", None),
            P("sp", None, "tp"),
            P("sp", None, "tp"),
            P("sp", "tp", None),
            P("sp", "tp"),
            P("sp", "tp"),
            P("sp", "tp"),
            P("sp", "tp"),
            P("sp", "tp"),
            P("sp", "tp"),
            P("sp", "tp", None, None),
        ),
        out_specs=(
            P("sp", None, "tp"),
            P("sp", None, "tp"),
            P("sp", "tp", None),
            P("sp", "tp"),
            P("sp", "tp"),
            P("sp", "tp"),
            P("sp", "tp"),
            P("sp", "tp"),
        ),
        check_vma=False,
    )
```

profile of v0, /device:TPU:0, one launch (start us, length us, event | category | flops | bytes accessed | tf_op | source)
XLA Modules:
  0.0 320.2 jit_solution(13305534653315224760)
XLA Ops:
  15.0 19.2 %all_to_all.33 = bf16[8,48,512]{2,1,0:T(8,128)(2,1)} all-to-all(bf16[8,48,512]{2,1,0:T(8,128)(2,1)S(1)} %bitcast.230), channel_id=1, replica_groups=mesh['sp'=8,'tp'=4] {'sp'}, dimensions={0} | all-to-all | bytes 786432 | tf_op jit(solution)/shard_map/all_to_all | solution.py:169
  35.0 15.1 %all_to_all.34 = bf16[8,48,512]{2,1,0:T(8,128)(2,1)} all-to-all(bf16[8,48,512]{2,1,0:T(8,128)(2,1)S(1)} %bitcast.231), channel_id=1, replica_groups=mesh['sp'=8,'tp'=4] {'sp'}, dimensions={0} | all-to-all | bytes 786432 | tf_op jit(solution)/shard_map/all_to_all | solution.py:172
  50.2 2.6 all-gather.8.cloned.1.call-done
  52.7 4.0 %fusion.12 = f32[384,512]{1,0:T(8,128)} fusion(bf16[1,2048,512]{2,1,0:T(8,128)(2,1)} %param.27, bf16[1,384,2048]{2,1,0:T(8,128)(2,1)} %all-gather.8.cloned.1.call-done), kind=kOutput, calls=%fused_computation.29 | convolution fusion | flops 805306368 | bytes 4456448 | tf_op jit(solution)/shard_map/erd,edf->erf/dot_general | solution.py:187
  58.6 15.3 %all-gather.10.cloned.1.call-done = bf16[1,384,2048]{2,1,0:T(8,128)(2,1)} async-done(((bf16[1,384,512]{2,1,0:T(8,128)(2,1)}), bf16[1,384,2048]{2,1,0:T(8,128)(2,1)}) %all-gather.10.cloned.1.call-update) | async-done | bytes 1572880 | tf_op jit(solution)/shard_map/all_gather | solution.py:182
  74.0 3.7 %multiply_convert_fusion.1 = (bf16[384,512]{1,0:T(8,128)(2,1)S(1)}, bf16[384,512]{1,0:T(8,128)(2,1)S(1)}) fusion(f32[384,512]{1,0:T(8,128)} %fusion.9, f32[384,512]{1,0:T(8,128)} %fusion.12, bf16[1,512,2048]{2,1,0:T(8,128)(2,1)} %param.28, bf16[1,384,2048]{2,1,0:T(8,128)(2,1)} %all-gather.10.cloned.1.call-done), kind=kOutput, calls=%fused_computation.64 | convolution fusion | flops 807862272 | bytes 6029312 | tf_op jit(solution)/shard_map/erd,efd->erf/dot_general | solution.py:190
  82.3 27.6 %reduce-scatter.3.cloned.1.call-done = bf16[1,384,512]{2,1,0:T(8,128)(2,1)} async-done(((bf16[1,384,2048]{2,1,0:T(8,128)(2,1)}), bf16[1,384,512]{2,1,0:T(8,128)(2,1)}) %reduce-scatter.3.cloned.1.call-update) | async-done | bytes 393232 | tf_op jit(solution)/shard_map/reduce_scatter | solution.py:212
  112.0 3.0 reduce.9
  116.1 5.6 %all-to-all-start.2 = ((bf16[8,2,12288]{2,1,0:T(2,128)(2,1)}), bf16[8,2,12288]{2,1,0:T(2,128)(2,1)S(1)}, u32[]{:S(2)}, u32[]{:S(2)}) async-start(bf16[8,2,12288]{2,1,0:T(2,128)(2,1)} %reshape.320), calls=%async_computation.3 | async-start | bytes 786432 | tf_op jit(solution)/shard_map/all_to_all | solution.py:216
  123.5 21.2 %all-to-all-done.2 = bf16[8,2,12288]{2,1,0:T(2,128)(2,1)S(1)} async-done(((bf16[8,2,12288]{2,1,0:T(2,128)(2,1)}), bf16[8,2,12288]{2,1,0:T(2,128)(2,1)S(1)}, u32[]{:S(2)}, u32[]{:S(2)}) %all-to-all-start.2) | async-done | bytes 393248 | tf_op jit(solution)/shard_map/all_to_all | solution.py:216
  145.4 6.9 %all_gather.24 = bf16[128,2048]{1,0:T(8,128)(2,1)S(1)} all-gather(bf16[128,512]{1,0:T(8,128)(2,1)S(1)} %convolution_convert_fusion.6), channel_id=1, replica_groups=mesh['sp'=8,'tp'=4] {'tp'}, dimensions={1}, use_global_device_ids=true | all-gather | bytes 655360 | tf_op jit(solution)/shard_map/all_gather | solution.py:218
  153.3 10.2 %all-gather.12.cloned.1.call-done = bf16[2048,1024]{1,0:T(8,128)(2,1)} async-done(((bf16[256,1024]{1,0:T(8,128)(2,1)}), bf16[2048,1024]{1,0:T(8,128)(2,1)}) %all-gather.12.cloned.1.call-update) | async-done | bytes 4194320 | tf_op jit(solution)/shard_map/all_gather | solution.py:243
  163.5 3.1 convolution_convert_fusion.5
  174.3 19.4 %all-gather.2 = bf16[8,4,128]{2,1,0:T(4,128)(2,1)} all-gather(bf16[1,4,128]{2,1,0:T(4,128)(2,1)S(1)} %fusion.47), channel_id=3, replica_groups=mesh['sp'=8,'tp'=4] {'sp'}, dimensions={0}, use_global_device_ids=true | all-gather | bytes 9216 | tf_op jit(solution)/shard_map/all_gather | solution.py:19
  195.8 4.5 %convolution_convert_fusion = bf16[2048,1024]{1,0:T(8,128)(2,1)} fusion(bf16[128,1024]{1,0:T(8,128)(2,1)S(1)} %copy-done.25, bf16[128,2048]{1,0:T(8,128)(2,1)S(1)} %all_gather.24, bf16[128,2048]{1,0:T(8,128)(2,1)} %param.23, f32[128]{0:T(128)} %copy-done.30, f32[2048]{0:T(1024)S(1)} %copy-done.26, f32[128]{0:T(128)} %copy-done.29, ...), kind=kOutput, calls=%fused_computation.15 | convolution fusion | flops 541589504 | bytes 6038528 | tf_op jit(solution)/shard_map/dot_general | solution.py:233
  201.3 9.4 %fusion = (f32[4,2,64,64]{3,2,1,0:T(8,128)}, f32[4,2,64,128,64]{3,4,2,1,0:T(8,128)}) fusion(f32[4,2,128,64]{2,3,1,0:T(8,128)S(1)} %bitcast.214, f32[4,2,128,64]{2,3,1,0:T(8,128)S(1)} %bitcast.226, f32[4,2,64,128]{3,2,1,0:T(8,128)S(1)} %reduce_window_sum.50, pred[64,64]{1,0:T(8,128)(4,1)S(1)} %iota_compare_fusion.2), kind=kLoop, calls=%fused_computation.9 | loop fusion | flops 20938752 | bytes 17698816 | tf_op jit(solution)/shard_map/vmap(ntd,nsd,ntsd->nts)/dot_general | solution.py:81
  211.3 4.5 %fusion.4 = bf16[1,2048,512]{2,1,0:T(8,128)(2,1)} fusion(bf16[384,512]{1,0:T(8,128)(2,1)} %copy-done.21, bf16[1,384,2048]{2,1,0:T(8,128)(2,1)} %all-gather.8.cloned.1.call-done), kind=kOutput, calls=%fused_computation.21 | convolution fusion | flops 806354944 | bytes 4063232 | tf_op jit(solution)/shard_map/erd,erf->edf/dot_general | solution.py:201
  215.9 2.6 fusion.3
  218.5 2.7 fusion.5
  222.8 15.1 %fusion.1 = f32[4,2,64,128]{3,2,1,0:T(8,128)S(1)} fusion(f32[4,2,64,128,64]{3,4,2,1,0:T(8,128)} %get-tuple-element.416, f32[4,2,64,128]{3,2,1,0:T(8,128)S(1)} %bitcast.215, f32[4,2,64,64]{3,2,1,0:T(8,128)S(1)} %copy.217), kind=kLoop, calls=%fused_computation.11 | loop fusion | flops 12517376 | bytes 17432576 | tf_op jit(solution)/shard_map/vmap(nts,nsd,ntsd->ntd)/dot_general | solution.py:84
  239.4 6.3 %multiply_reduce_fusion = f32[4,2,64,128]{3,2,1,0:T(8,128)} fusion(f32[4,2,64,64]{3,2,1,0:T(8,128)S(1)} %fusion.51, f32[4,2,64,128]{3,2,1,0:T(8,128)S(1)} %bitcast.227, f32[4,2,64,128]{3,2,1,0:T(8,128)S(1)} %reduce_window_sum.50, pred[64,64]{1,0:T(8,128)(4,1)S(1)} %iota_compare_fusion.2), kind=kLoop, calls=%fused_computation.12 | loop fusion | flops 20905984 | bytes 921600 | tf_op jit(solution)/shard_map/vmap(nts,ntd,ntsd->nsd)/dot_general | solution.py:88
  245.8 12.8 %while.44 = (s32[]{:T(128)}, f32[4,128,256]{2,1,0:T(8,128)S(1)}, s32[]{:T(128)}, bf16[8,4,128,256]{3,2,1,0:T(8,128)(2,1)}, bf16[8,4,128]{2,1,0:T(4,128)(2,1)}, /*index=5*/s32[]{:T(128)}, s32[]{:T(128)}, s32[]{:T(128)}, s32[]{:T(128)}) while((s32[]{:T(128)}, f32[4,128,256]{2,1,0:T(8,128)S(1)}, s32[]{:T(128)}, ...), condition=%wide.region_17.18_spmd, body=%wide.region_16.17_spmd.sunk | while | flops 393734 | bytes 1315987 | solution.py:34
  258.6 2.7 multiply_subtract_fusion
  268.3 42.4 %reduce-scatter.5.cloned.1.call-done = bf16[256,1024]{1,0:T(8,128)(2,1)} async-done(((bf16[2048,1024]{1,0:T(8,128)(2,1)}), bf16[256,1024]{1,0:T(8,128)(2,1)}) %reduce-scatter.5.cloned.1.call-update) | async-done | bytes 524304 | tf_op jit(solution)/shard_map/reduce_scatter | solution.py:232
  (188 shorter events, 59.0 us)
Async XLA Ops:
  8.0 48.8 %copy-start = (bf16[1,2048,512]{2,1,0:T(8,128)(2,1)S(1)}, bf16[1,2048,512]{2,1,0:T(8,128)(2,1)}, u32[]{:S(2)}) copy-start(bf16[1,2048,512]{2,1,0:T(8,128)(2,1)} %param.26) | copy-start | bytes 6291460
  8.0 44.7 %all-gather.8.cloned.1.call-start = ((), (), s32[]{:S(2)}) async-start(), calls=%async_computation.5 | async-start | bytes 1966080 | tf_op jit(solution)/shard_map/all_gather | solution.py:181
  10.2 24.1 %copy-start.31 = (f32[128,2]{0,1:T(2,128)S(1)}, f32[128,2]{0,1:T(2,128)}, u32[]{:S(2)}) copy-start(f32[128,2]{0,1:T(2,128)} %param.25) | copy-start | bytes 3076
  10.5 24.2 %copy-start.9 = (bf16[128,2048]{1,0:T(8,128)(2,1)S(1)}, bf16[128,2048]{1,0:T(8,128)(2,1)}, u32[]{:S(2)}) copy-start(bf16[128,2048]{1,0:T(8,128)(2,1)} %param.23) | copy-start | bytes 1572868
  11.3 23.7 %copy-start.19 = (pred[384,128]{1,0:T(8,128)(4,1)}, pred[384,128]{1,0:T(8,128)(4,1)S(1)}, u32[]{:S(2)}) copy-start(pred[384,128]{1,0:T(8,128)(4,1)S(1)} %fusion.34) | copy-start | bytes 147460
  34.2 39.7 %all-gather.10.cloned.1.call-start = ((), (), s32[]{:S(2)}) async-start(), calls=%async_computation.6 | async-start | bytes 1966080 | tf_op jit(solution)/shard_map/all_gather | solution.py:182
  50.1 59.7 %reduce-scatter.3.cloned.1.call-start = ((), (), s32[]{:S(2)}) async-start(), calls=%async_computation.7 | async-start | bytes 1966080 | tf_op jit(solution)/shard_map/reduce_scatter | solution.py:212
  81.7 81.7 %all-gather.12.cloned.1.call-start = ((), (), s32[]{:S(2)}) async-start(), calls=%async_computation.9 | async-start | bytes 4718592 | tf_op jit(solution)/shard_map/all_gather | solution.py:243
  82.3 39.5 %copy-start.24 = (f32[128,512]{1,0:T(8,128)S(1)}, f32[128,512]{1,0:T(8,128)}, u32[]{:S(2)}) copy-start(f32[128,512]{1,0:T(8,128)} %param.34) | copy-start | bytes 786436
  112.0 10.8 %copy-start.17 = (bf16[128,512]{1,0:T(8,128)(2,1)S(1)}, bf16[128,512]{1,0:T(8,128)(2,1)}, u32[]{:S(2)}) copy-start(bf16[128,512]{1,0:T(8,128)(2,1)} %param.31) | copy-start | bytes 393220
  116.1 29.0 %copy-start.20 = (pred[384,128]{1,0:T(8,128)(4,1)S(1)}, pred[384,128]{1,0:T(8,128)(4,1)}, u32[]{:S(2)}) copy-start(pred[384,128]{1,0:T(8,128)(4,1)} %copy-done.19) | copy-start | bytes 147460
  116.1 28.6 %all-to-all-start.2 = ((bf16[8,2,12288]{2,1,0:T(2,128)(2,1)}), bf16[8,2,12288]{2,1,0:T(2,128)(2,1)S(1)}, u32[]{:S(2)}, u32[]{:S(2)}) async-start(bf16[8,2,12288]{2,1,0:T(2,128)(2,1)} %reshape.320), calls=%async_computation.3 | async-start | bytes 786432 | tf_op jit(solution)/shard_map/all_to_all | solution.py:216
  121.7 124.0 %all-gather.14.cloned.1.call-start = ((), (), s32[]{:S(2)}) async-start(), calls=%async_computation.10 | async-start | bytes 2359296 | tf_op jit(solution)/shard_map/all_gather | solution.py:19
  153.3 13.3 %copy-start.30 = (f32[128]{0:T(128)}, f32[128]{0:T(128)S(1)}, u32[]{:S(2)}) copy-start(f32[128]{0:T(128)S(1)} %broadcast_multiply_fusion) | copy-start | bytes 1540
  171.6 22.1 %copy-start.16 = (bf16[128,512]{1,0:T(8,128)(2,1)S(1)}, bf16[128,512]{1,0:T(8,128)(2,1)}, u32[]{:S(2)}) copy-start(bf16[128,512]{1,0:T(8,128)(2,1)} %param.32) | copy-start | bytes 393220
  172.3 23.5 %copy-start.25 = (bf16[128,1024]{1,0:T(8,128)(2,1)S(1)}, bf16[128,1024]{1,0:T(8,128)(2,1)}, u32[]{:S(2)}) copy-start(bf16[128,1024]{1,0:T(8,128)(2,1)} %param.30) | copy-start | bytes 786436
  172.4 138.4 %reduce-scatter.5.cloned.1.call-start = ((), (), s32[]{:S(2)}) async-start(), calls=%async_computation.8 | async-start | bytes 4718592 | tf_op jit(solution)/shard_map/reduce_scatter | solution.py:232
  173.6 26.7 %copy-start.5 = (bf16[4,128,256]{2,1,0:T(8,128)(2,1)}, bf16[4,128,256]{2,1,0:T(8,128)(2,1)S(1)}, u32[]{:S(2)}) copy-start(bf16[4,128,256]{2,1,0:T(8,128)(2,1)S(1)} %copy.213) | copy-start | bytes 786436
  222.8 15.1 %copy-start.8 = (f32[2,4,128,256]{3,2,1,0:T(8,128)S(1)}, f32[2,4,128,256]{3,2,1,0:T(8,128)}, u32[]{:S(2)}) copy-start(f32[2,4,128,256]{3,2,1,0:T(8,128)} %copy-done.7) | copy-start | bytes 3145732
  239.4 19.2 %copy-start.15 = (f32[16,4,8,128]{3,2,1,0:T(8,128)S(1)}, f32[16,4,8,128]{3,2,1,0:T(8,128)}, u32[]{:S(2)}) copy-start(f32[16,4,8,128]{3,2,1,0:T(8,128)} %multiply_bitcast_fusion) | copy-start | bytes 786436
  245.7 12.9 %copy-start.4 = (f32[2,4,128,256]{3,2,1,0:T(8,128)S(1)}, f32[2,4,128,256]{3,2,1,0:T(8,128)}, u32[]{:S(2)}) copy-start(f32[2,4,128,256]{3,2,1,0:T(8,128)} %get-tuple-element.225) | copy-start | bytes 3145732
  245.7 12.9 %copy-start.14 = (f32[16,4,8,128]{3,2,1,0:T(8,128)S(1)}, f32[16,4,8,128]{3,2,1,0:T(8,128)}, u32[]{:S(2)}) copy-start(f32[16,4,8,128]{3,2,1,0:T(8,128)} %convert_bitcast_fusion) | copy-start | bytes 786436
  245.7 12.9 %copy-start.27 = (f32[4,2,128]{2,0,1:T(4,128)S(1)}, f32[4,2,128]{2,0,1:T(4,128)}, u32[]{:S(2)}) copy-start(f32[4,2,128]{2,0,1:T(4,128)} %copy.222) | copy-start | bytes 12292
  263.7 49.1 %copy-start.1 = (bf16[1,2048,512]{2,1,0:T(8,128)(2,1)S(1)}, bf16[1,2048,512]{2,1,0:T(8,128)(2,1)}, u32[]{:S(2)}) copy-start(bf16[1,2048,512]{2,1,0:T(8,128)(2,1)} %param.26) | copy-start | bytes 6291460
  (20 other events, 63.7 us)
Sparse Core Ops, SparseCore 0:
  34.4 18.3 all-gather.7
  54.3 19.6 all-gather.9
  81.8 27.9 reduce-scatter.2
Sparse Core Ops, SparseCore 1:
  84.3 79.1 all-gather.11
  172.4 47.9 all-gather.13
  223.9 86.8 reduce-scatter.4
where the time goes:
time: 321 us; the launch traced here: 320 us
  waiting for transfers between devices  120 us (37%)
  blocking collectives  60.6 us (19%)
  other arithmetic  60 us (19%)
  matrix products  42 us (13%)
  between operations  16.1 us (5%)
  local copies, waits for them, and re-layouts  15.2 us (5%)
  starting transfers between devices  5.89 us (2%)
    reduce_scatter x1, waiting for transfers between devices, on_device(): lax.psum_scatter(lax.dot_general(resid_cols, mixed, (((0,), (0,)), ((), (...  42.4 us
    reduce_scatter x1, waiting for transfers between devices, on_device(): lax.psum_scatter(partial_short, 'tp', scatter_dimension=2, tiled=True)  27.6 us
    all_to_all x1, waiting for transfers between devices, on_device(): lax.all_to_all(summed, 'sp', split_axis=1, concat_axis=0, tiled=True)  21.2 us
    all_gather x1, blocking collectives, entering(): lax.all_gather(a.astype(kind), axis)  19.4 us
    all_to_all x1, blocking collectives, on_device(): lax.all_to_all(rows_in.reshape(experts, capacity, -1), 'sp', split_axis=0...  19.2 us
    all_gather x1, waiting for transfers between devices, on_device(): lax.all_gather(arrived[1], 'tp', axis=2, tiled=True)  15.3 us
    dot_general x1, other arithmetic, span_backward(): jnp.einsum('nts,nsd,ntsd->ntd', grad_scores, key_blk, decays, precision=h...  15.1 us
    all_to_all x1, blocking collectives, on_device(): lax.all_to_all(rows_cot.astype(jnp.bfloat16).reshape(experts, capacity, -...  15.1 us
  transfers between devices with their start and end apart: 7, of which 6 were waited for; matrix products, arithmetic and copies ran while one was open for 28% of the time, Pallas kernels for 0%

commit v1 on v0

--- a/solution.py
+++ b/solution.py
@@ -9,6 +9,13 @@
 BLOCK = 64
 epsilon = 1e-06
 highest = lax.Precision.HIGHEST
+
+
+def exchange_blocks(block, axis, split, join):
+    peers = lax.axis_size(axis)
+    tiles = jnp.stack(jnp.split(block, peers, axis=split), axis=0)
+    tiles = lax.all_to_all(tiles, axis, split_axis=0, concat_axis=0)
+    return jnp.concatenate(tiles, axis=join)
 
 
 def entering(array, axis, join, neutral):
@@ -166,9 +173,7 @@
         * slot_weight[:, None]
     )
     arrived = (
-        lax.all_to_all(
-            rows_in.reshape(experts, capacity, -1), "sp", split_axis=0, concat_axis=1, tiled=True
-        ),
+        exchange_blocks(rows_in.reshape(experts, capacity, -1), "sp", 0, 1),
         lax.all_to_all(
             rows_cot.astype(jnp.bfloat16).reshape(experts, capacity, -1),
             "sp",

time: 321 us -> 321 us (level)
  no operation moved by 1% of the time
where the time goes in v1:
time: 321 us; the launch traced here: 320 us
  waiting for transfers between devices  120 us (37%)
  blocking collectives  60.6 us (19%)
  other arithmetic  60 us (19%)
  matrix products  42 us (13%)
  between operations  16.2 us (5%)
  local copies, waits for them, and re-layouts  15.3 us (5%)
  starting transfers between devices  5.89 us (2%)
    reduce_scatter x1, waiting for transfers between devices, on_device(): lax.psum_scatter(lax.dot_general(resid_cols, mixed, (((0,), (0,)), ((), (...  42.4 us
    reduce_scatter x1, waiting for transfers between devices, on_device(): lax.psum_scatter(partial_short, 'tp', scatter_dimension=2, tiled=True)  27.5 us
    all_to_all x1, waiting for transfers between devices, on_device(): lax.all_to_all(summed, 'sp', split_axis=1, concat_axis=0, tiled=True)  21.2 us
    all_gather x1, blocking collectives, entering(): lax.all_gather(a.astype(kind), axis)  19.4 us
    all_to_all x1, blocking collectives, exchange_blocks(): tiles = lax.all_to_all(tiles, axis, split_axis=0, concat_axis=0)  19.2 us
    all_gather x1, waiting for transfers between devices, on_device(): lax.all_gather(arrived[1], 'tp', axis=2, tiled=True)  15.3 us
    dot_general x1, other arithmetic, span_backward(): jnp.einsum('nts,nsd,ntsd->ntd', grad_scores, key_blk, decays, precision=h...  15.1 us
    all_to_all x1, blocking collectives, on_device(): lax.all_to_all(rows_cot.astype(jnp.bfloat16).reshape(experts, capacity, -...  15.1 us
  transfers between devices with their start and end apart: 7, of which 6 were waited for; matrix products, arithmetic and copies ran while one was open for 28% of the time, Pallas kernels for 0%

profile of v1, /device:TPU:0, one launch (start us, length us, event | category | flops | bytes accessed | tf_op | source)
XLA Modules:
  0.0 320.3 jit_solution(5627342192317848681)
XLA Ops:
  15.1 19.2 %all_to_all.26 = bf16[8,1,48,512]{3,2,1,0:T(8,128)(2,1)} all-to-all(bf16[8,1,48,512]{3,2,1,0:T(8,128)(2,1)S(1)} %fusion.44), channel_id=1, replica_groups=mesh['sp'=8,'tp'=4] {'sp'}, dimensions={0} | all-to-all | bytes 786432 | tf_op jit(solution)/shard_map/all_to_all | solution.py:17
  35.1 15.1 %all_to_all.27 = bf16[8,48,512]{2,1,0:T(8,128)(2,1)} all-to-all(bf16[8,48,512]{2,1,0:T(8,128)(2,1)S(1)} %bitcast.261), channel_id=1, replica_groups=mesh['sp'=8,'tp'=4] {'sp'}, dimensions={0} | all-to-all | bytes 786432 | tf_op jit(solution)/shard_map/all_to_all | solution.py:177
  50.2 2.6 all-gather.8.cloned.1.call-done
  52.8 4.0 %fusion.12 = f32[384,512]{1,0:T(8,128)} fusion(bf16[1,2048,512]{2,1,0:T(8,128)(2,1)} %param.27, bf16[1,384,2048]{2,1,0:T(8,128)(2,1)} %all-gather.8.cloned.1.call-done), kind=kOutput, calls=%fused_computation.29 | convolution fusion | flops 805306368 | bytes 4456448 | tf_op jit(solution)/shard_map/erd,edf->erf/dot_general | solution.py:192
  58.7 15.3 %all-gather.10.cloned.1.call-done = bf16[1,384,2048]{2,1,0:T(8,128)(2,1)} async-done(((bf16[1,384,512]{2,1,0:T(8,128)(2,1)}), bf16[1,384,2048]{2,1,0:T(8,128)(2,1)}) %all-gather.10.cloned.1.call-update) | async-done | bytes 1572880 | tf_op jit(solution)/shard_map/all_gather | solution.py:187
  74.0 3.7 %multiply_convert_fusion.1 = (bf16[384,512]{1,0:T(8,128)(2,1)S(1)}, bf16[384,512]{1,0:T(8,128)(2,1)S(1)}) fusion(f32[384,512]{1,0:T(8,128)} %fusion.9, f32[384,512]{1,0:T(8,128)} %fusion.12, bf16[1,512,2048]{2,1,0:T(8,128)(2,1)} %param.28, bf16[1,384,2048]{2,1,0:T(8,128)(2,1)} %all-gather.10.cloned.1.call-done), kind=kOutput, calls=%fused_computation.64 | convolution fusion | flops 807862272 | bytes 6029312 | tf_op jit(solution)/shard_map/erd,efd->erf/dot_general | solution.py:195
  82.4 27.5 %reduce-scatter.3.cloned.1.call-done = bf16[1,384,512]{2,1,0:T(8,128)(2,1)} async-done(((bf16[1,384,2048]{2,1,0:T(8,128)(2,1)}), bf16[1,384,512]{2,1,0:T(8,128)(2,1)}) %reduce-scatter.3.cloned.1.call-update) | async-done | bytes 393232 | tf_op jit(solution)/shard_map/reduce_scatter | solution.py:217
  112.0 3.0 reduce.9
  116.1 5.6 %all-to-all-start.2 = ((bf16[8,2,12288]{2,1,0:T(2,128)(2,1)}), bf16[8,2,12288]{2,1,0:T(2,128)(2,1)S(1)}, u32[]{:S(2)}, u32[]{:S(2)}) async-start(bf16[8,2,12288]{2,1,0:T(2,128)(2,1)} %reshape.334), calls=%async_computation.3 | async-start | bytes 786432 | tf_op jit(solution)/shard_map/all_to_all | solution.py:221
  123.5 21.2 %all-to-all-done.2 = bf16[8,2,12288]{2,1,0:T(2,128)(2,1)S(1)} async-done(((bf16[8,2,12288]{2,1,0:T(2,128)(2,1)}), bf16[8,2,12288]{2,1,0:T(2,128)(2,1)S(1)}, u32[]{:S(2)}, u32[]{:S(2)}) %all-to-all-start.2) | async-done | bytes 393248 | tf_op jit(solution)/shard_map/all_to_all | solution.py:221
  145.4 6.9 %all_gather.24 = bf16[128,2048]{1,0:T(8,128)(2,1)S(1)} all-gather(bf16[128,512]{1,0:T(8,128)(2,1)S(1)} %convolution_convert_fusion.6), channel_id=1, replica_groups=mesh['sp'=8,'tp'=4] {'tp'}, dimensions={1}, use_global_device_ids=true | all-gather | bytes 655360 | tf_op jit(solution)/shard_map/all_gather | solution.py:223
  153.4 10.2 %all-gather.12.cloned.1.call-done = bf16[2048,1024]{1,0:T(8,128)(2,1)} async-done(((bf16[256,1024]{1,0:T(8,128)(2,1)}), bf16[2048,1024]{1,0:T(8,128)(2,1)}) %all-gather.12.cloned.1.call-update) | async-done | bytes 4194320 | tf_op jit(solution)/shard_map/all_gather | solution.py:248
  163.5 3.1 convolution_convert_fusion.5
  174.4 19.4 %all-gather.2 = bf16[8,4,128]{2,1,0:T(4,128)(2,1)} all-gather(bf16[1,4,128]{2,1,0:T(4,128)(2,1)S(1)} %fusion.55), channel_id=3, replica_groups=mesh['sp'=8,'tp'=4] {'sp'}, dimensions={0}, use_global_device_ids=true | all-gather | bytes 9216 | tf_op jit(solution)/shard_map/all_gather | solution.py:26
  195.9 4.5 %convolution_convert_fusion = bf16[2048,1024]{1,0:T(8,128)(2,1)} fusion(bf16[128,1024]{1,0:T(8,128)(2,1)S(1)} %copy-done.25, bf16[128,2048]{1,0:T(8,128)(2,1)S(1)} %all_gather.24, bf16[128,2048]{1,0:T(8,128)(2,1)} %param.23, f32[128]{0:T(128)} %copy-done.30, f32[2048]{0:T(1024)S(1)} %copy-done.26, f32[128]{0:T(128)} %copy-done.29, ...), kind=kOutput, calls=%fused_computation.15 | convolution fusion | flops 541589504 | bytes 6038528 | tf_op jit(solution)/shard_map/dot_general | solution.py:238
  201.4 9.4 %fusion = (f32[4,2,64,64]{3,2,1,0:T(8,128)}, f32[4,2,64,128,64]{3,4,2,1,0:T(8,128)}) fusion(f32[4,2,128,64]{2,3,1,0:T(8,128)S(1)} %bitcast.245, f32[4,2,128,64]{2,3,1,0:T(8,128)S(1)} %bitcast.257, f32[4,2,64,128]{3,2,1,0:T(8,128)S(1)} %reduce_window_sum.50, pred[64,64]{1,0:T(8,128)(4,1)S(1)} %iota_compare_fusion.2), kind=kLoop, calls=%fused_computation.9 | loop fusion | flops 20938752 | bytes 17698816 | tf_op jit(solution)/shard_map/vmap(ntd,nsd,ntsd->nts)/dot_general | solution.py:88
  211.3 4.5 %fusion.4 = bf16[1,2048,512]{2,1,0:T(8,128)(2,1)} fusion(bf16[384,512]{1,0:T(8,128)(2,1)} %copy-done.21, bf16[1,384,2048]{2,1,0:T(8,128)(2,1)} %all-gather.8.cloned.1.call-done), kind=kOutput, calls=%fused_computation.21 | convolution fusion | flops 806354944 | bytes 4063232 | tf_op jit(solution)/shard_map/erd,erf->edf/dot_general | solution.py:206
  215.9 2.6 fusion.3
  218.6 2.7 fusion.5
  222.9 15.1 %fusion.1 = f32[4,2,64,128]{3,2,1,0:T(8,128)S(1)} fusion(f32[4,2,64,128,64]{3,4,2,1,0:T(8,128)} %get-tuple-element.416, f32[4,2,64,128]{3,2,1,0:T(8,128)S(1)} %bitcast.246, f32[4,2,64,64]{3,2,1,0:T(8,128)S(1)} %copy.217), kind=kLoop, calls=%fused_computation.11 | loop fusion | flops 12517376 | bytes 17432576 | tf_op jit(solution)/shard_map/vmap(nts,nsd,ntsd->ntd)/dot_general | solution.py:91
  239.5 6.3 %multiply_reduce_fusion = f32[4,2,64,128]{3,2,1,0:T(8,128)} fusion(f32[4,2,64,64]{3,2,1,0:T(8,128)S(1)} %fusion.59, f32[4,2,64,128]{3,2,1,0:T(8,128)S(1)} %bitcast.258, f32[4,2,64,128]{3,2,1,0:T(8,128)S(1)} %reduce_window_sum.50, pred[64,64]{1,0:T(8,128)(4,1)S(1)} %iota_compare_fusion.2), kind=kLoop, calls=%fused_computation.12 | loop fusion | flops 20905984 | bytes 921600 | tf_op jit(solution)/shard_map/vmap(nts,ntd,ntsd->nsd)/dot_general | solution.py:95
  245.8 12.8 %while.44 = (s32[]{:T(128)}, f32[4,128,256]{2,1,0:T(8,128)S(1)}, s32[]{:T(128)}, bf16[8,4,128,256]{3,2,1,0:T(8,128)(2,1)}, bf16[8,4,128]{2,1,0:T(4,128)(2,1)}, /*index=5*/s32[]{:T(128)}, s32[]{:T(128)}, s32[]{:T(128)}, s32[]{:T(128)}) while((s32[]{:T(128)}, f32[4,128,256]{2,1,0:T(8,128)S(1)}, s32[]{:T(128)}, ...), condition=%wide.region_17.18_spmd, body=%wide.region_16.17_spmd.sunk | while | flops 393734 | bytes 1315987 | solution.py:41
  258.7 2.7 multiply_subtract_fusion
  268.4 42.4 %reduce-scatter.5.cloned.1.call-done = bf16[256,1024]{1,0:T(8,128)(2,1)} async-done(((bf16[2048,1024]{1,0:T(8,128)(2,1)}), bf16[256,1024]{1,0:T(8,128)(2,1)}) %reduce-scatter.5.cloned.1.call-update) | async-done | bytes 524304 | tf_op jit(solution)/shard_map/reduce_scatter | solution.py:237
  (196 shorter events, 59.0 us)
Async XLA Ops:
  8.0 48.8 %copy-start = (bf16[1,2048,512]{2,1,0:T(8,128)(2,1)S(1)}, bf16[1,2048,512]{2,1,0:T(8,128)(2,1)}, u32[]{:S(2)}) copy-start(bf16[1,2048,512]{2,1,0:T(8,128)(2,1)} %param.26) | copy-start | bytes 6291460
  8.0 44.8 %all-gather.8.cloned.1.call-start = ((), (), s32[]{:S(2)}) async-start(), calls=%async_computation.5 | async-start | bytes 1966080 | tf_op jit(solution)/shard_map/all_gather | solution.py:186
  11.2 23.6 %copy-start.19 = (pred[384,128]{1,0:T(8,128)(4,1)}, pred[384,128]{1,0:T(8,128)(4,1)S(1)}, u32[]{:S(2)}) copy-start(pred[384,128]{1,0:T(8,128)(4,1)S(1)} %fusion.34) | copy-start | bytes 147460
  12.5 21.9 %copy-start.31 = (f32[128,2]{0,1:T(2,128)S(1)}, f32[128,2]{0,1:T(2,128)}, u32[]{:S(2)}) copy-start(f32[128,2]{0,1:T(2,128)} %param.25) | copy-start | bytes 3076
  12.5 22.3 %copy-start.9 = (bf16[128,2048]{1,0:T(8,128)(2,1)S(1)}, bf16[128,2048]{1,0:T(8,128)(2,1)}, u32[]{:S(2)}) copy-start(bf16[128,2048]{1,0:T(8,128)(2,1)} %param.23) | copy-start | bytes 1572868
  34.3 39.7 %all-gather.10.cloned.1.call-start = ((), (), s32[]{:S(2)}) async-start(), calls=%async_computation.6 | async-start | bytes 1966080 | tf_op jit(solution)/shard_map/all_gather | solution.py:187
  50.2 59.7 %reduce-scatter.3.cloned.1.call-start = ((), (), s32[]{:S(2)}) async-start(), calls=%async_computation.7 | async-start | bytes 1966080 | tf_op jit(solution)/shard_map/reduce_scatter | solution.py:217
  81.8 81.7 %all-gather.12.cloned.1.call-start = ((), (), s32[]{:S(2)}) async-start(), calls=%async_computation.9 | async-start | bytes 4718592 | tf_op jit(solution)/shard_map/all_gather | solution.py:248
  82.4 39.4 %copy-start.24 = (f32[128,512]{1,0:T(8,128)S(1)}, f32[128,512]{1,0:T(8,128)}, u32[]{:S(2)}) copy-start(f32[128,512]{1,0:T(8,128)} %param.34) | copy-start | bytes 786436
  112.0 10.8 %copy-start.17 = (bf16[128,512]{1,0:T(8,128)(2,1)S(1)}, bf16[128,512]{1,0:T(8,128)(2,1)}, u32[]{:S(2)}) copy-start(bf16[128,512]{1,0:T(8,128)(2,1)} %param.31) | copy-start | bytes 393220
  116.1 29.0 %copy-start.20 = (pred[384,128]{1,0:T(8,128)(4,1)S(1)}, pred[384,128]{1,0:T(8,128)(4,1)}, u32[]{:S(2)}) copy-start(pred[384,128]{1,0:T(8,128)(4,1)} %copy-done.19) | copy-start | bytes 147460
  116.1 28.6 %all-to-all-start.2 = ((bf16[8,2,12288]{2,1,0:T(2,128)(2,1)}), bf16[8,2,12288]{2,1,0:T(2,128)(2,1)S(1)}, u32[]{:S(2)}, u32[]{:S(2)}) async-start(bf16[8,2,12288]{2,1,0:T(2,128)(2,1)} %reshape.334), calls=%async_computation.3 | async-start | bytes 786432 | tf_op jit(solution)/shard_map/all_to_all | solution.py:221
  121.8 124.0 %all-gather.14.cloned.1.call-start = ((), (), s32[]{:S(2)}) async-start(), calls=%async_computation.10 | async-start | bytes 2359296 | tf_op jit(solution)/shard_map/all_gather | solution.py:26
  153.3 13.3 %copy-start.30 = (f32[128]{0:T(128)}, f32[128]{0:T(128)S(1)}, u32[]{:S(2)}) copy-start(f32[128]{0:T(128)S(1)} %broadcast_multiply_fusion) | copy-start | bytes 1540
  171.7 22.1 %copy-start.16 = (bf16[128,512]{1,0:T(8,128)(2,1)S(1)}, bf16[128,512]{1,0:T(8,128)(2,1)}, u32[]{:S(2)}) copy-start(bf16[128,512]{1,0:T(8,128)(2,1)} %param.32) | copy-start | bytes 393220
  172.4 23.5 %copy-start.25 = (bf16[128,1024]{1,0:T(8,128)(2,1)S(1)}, bf16[128,1024]{1,0:T(8,128)(2,1)}, u32[]{:S(2)}) copy-start(bf16[128,1024]{1,0:T(8,128)(2,1)} %param.30) | copy-start | bytes 786436
  172.4 138.4 %reduce-scatter.5.cloned.1.call-start = ((), (), s32[]{:S(2)}) async-start(), calls=%async_computation.8 | async-start | bytes 4718592 | tf_op jit(solution)/shard_map/reduce_scatter | solution.py:237
  173.7 26.7 %copy-start.5 = (bf16[4,128,256]{2,1,0:T(8,128)(2,1)}, bf16[4,128,256]{2,1,0:T(8,128)(2,1)S(1)}, u32[]{:S(2)}) copy-start(bf16[4,128,256]{2,1,0:T(8,128)(2,1)S(1)} %copy.213) | copy-start | bytes 786436
  222.9 15.1 %copy-start.8 = (f32[2,4,128,256]{3,2,1,0:T(8,128)S(1)}, f32[2,4,128,256]{3,2,1,0:T(8,128)}, u32[]{:S(2)}) copy-start(f32[2,4,128,256]{3,2,1,0:T(8,128)} %copy-done.7) | copy-start | bytes 3145732
  239.5 19.2 %copy-start.15 = (f32[16,4,8,128]{3,2,1,0:T(8,128)S(1)}, f32[16,4,8,128]{3,2,1,0:T(8,128)}, u32[]{:S(2)}) copy-start(f32[16,4,8,128]{3,2,1,0:T(8,128)} %multiply_bitcast_fusion) | copy-start | bytes 786436
  245.8 12.9 %copy-start.4 = (f32[2,4,128,256]{3,2,1,0:T(8,128)S(1)}, f32[2,4,128,256]{3,2,1,0:T(8,128)}, u32[]{:S(2)}) copy-start(f32[2,4,128,256]{3,2,1,0:T(8,128)} %get-tuple-element.225) | copy-start | bytes 3145732
  245.8 12.9 %copy-start.14 = (f32[16,4,8,128]{3,2,1,0:T(8,128)S(1)}, f32[16,4,8,128]{3,2,1,0:T(8,128)}, u32[]{:S(2)}) copy-start(f32[16,4,8,128]{3,2,1,0:T(8,128)} %convert_bitcast_fusion) | copy-start | bytes 786436
  245.8 12.9 %copy-start.27 = (f32[4,2,128]{2,0,1:T(4,128)S(1)}, f32[4,2,128]{2,0,1:T(4,128)}, u32[]{:S(2)}) copy-start(f32[4,2,128]{2,0,1:T(4,128)} %copy.222) | copy-start | bytes 12292
  263.8 49.1 %copy-start.1 = (bf16[1,2048,512]{2,1,0:T(8,128)(2,1)S(1)}, bf16[1,2048,512]{2,1,0:T(8,128)(2,1)}, u32[]{:S(2)}) copy-start(bf16[1,2048,512]{2,1,0:T(8,128)(2,1)} %param.26) | copy-start | bytes 6291460
  (20 other events, 63.7 us)
Sparse Core Ops, SparseCore 0:
  34.4 18.3 all-gather.7
  54.4 19.6 all-gather.9
  81.9 27.9 reduce-scatter.2
Sparse Core Ops, SparseCore 1:
  84.4 79.1 all-gather.11
  172.5 47.9 all-gather.13
  224.0 86.8 reduce-scatter.4
